TPU v7x, 32 devices: a whole 2x2x4 slice. The times are simulated.
32 devices in a mesh: grp: 2 (over y), tp: 4 (over z), dp: 4 (over x, core).
Axes of the slice: x: 2, y: 2, z: 4, core: 2. Of those that a mesh axis runs over, the one named last changes fastest.
Arguments:
- tokens: bfloat16 [512, 4096], P('grp', 'dp'), parts along dimension 0, may hold values from -40 to 40
- sequence_lengths: int32 [512], P(('grp', 'dp')), parts along dimension 0, may hold values from 1 to 4096, 262144 in all
- recurrent_state: float32 [2, 512, 128, 128], P(None, ('grp', 'dp'), 'tp'), parts along dimension 1, may hold values from -1.8 to 1.8
- norm_weight: float32 [2, 4096], P(None, 'dp'), may hold values from 0.1 to 1.9
- input_weight: bfloat16 [2, 4096, 2048], P(None, 'dp', 'tp'), may hold values from -0.09375 to 0.09375
- gate_weight: bfloat16 [2, 4096, 2048], P(None, 'dp', 'tp'), may hold values from -0.09375 to 0.09375
- output_weight: bfloat16 [2, 2048, 4096], P(None, 'tp', 'dp'), may hold values from -0.125 to 0.125
- negated_real_rate: float32 [2, 8192], P(None, 'tp'), may hold values from 0.005 to 1
- frequency: float32 [2, 8192], P(None, 'tp'), may hold values from -4 to 4
- discrete_step: float32 [2, 128], P(None, 'tp'), may hold values from 0.02 to 0.5
- group_input_matrix: float32 [2, 128, 16, 128], P(None, 'tp'), may hold values from -1.5 to 1.5
- group_output_matrix: float32 [2, 128, 16, 128], P(None, 'tp'), may hold values from -0.5 to 0.5
- feedthrough_weight: float32 [2, 2048], P(None, 'tp'), may hold values from -3 to 3
- extra_log_decay: float32 [2, 128, 4096], P(None, 'tp'), may hold values from -0.7 to 0
Outputs:
- tokens_out: bfloat16 [512, 4096], P('grp', 'dp'), parts along dimension 0
- state_out: float32 [2, 512, 128, 128], P(None, ('grp', 'dp'), 'tp'), parts along dimension 1
There are 2 independent parts, one for each index of `grp`. A program takes and returns all parts, laid end to end along the dimension named above; an argument that names none is the same for every part. Nothing has to cross between parts.
Inputs may be any that keep to these rules, and one draw needn't show every extreme that they name: The newest token of a sequence stands at position sequence_lengths - 1.
All inputs are finite; a program needn't handle non-finite values. No bound on the sum of `sequence_lengths` on one device may be relied on, other than what follows from the above.
Results may differ from a plain program's by a relative error of at most 0.009.
Values may be sent and summed in bfloat16 or wider, within the bound.
A program may use at most 64 MiB of HBM per device.

v0:
```python
import jax
import jax.numpy as jnp
from jax import lax
from jax.sharding import PartitionSpec as P

D = 4096
STACKED_LAYERS = 2


TOP_PRECISION = lax.Precision.HIGHEST
NORM_EPS = 1e-06


def transition(decay_factor, angular_frequency, step_width):
    log_mag = -decay_factor * step_width[:, None]
    turn = angular_frequency * step_width[:, None]
    magnitude = jnp.exp(log_mag)
    discrete_real = magnitude * jnp.cos(turn)
    discrete_imaginary = magnitude * jnp.sin(turn)
    half_sine = jnp.sin(0.5 * turn)
    numer_re = jnp.expm1(log_mag) * jnp.cos(turn) - 2.0 * half_sine * half_sine
    denom = decay_factor * decay_factor + angular_frequency * angular_frequency
    drive_re = (-numer_re * decay_factor + discrete_imaginary * angular_frequency) / denom
    drive_im = (-discrete_imaginary * decay_factor - numer_re * angular_frequency) / denom
    return (discrete_real, discrete_imaginary, drive_re, drive_im)


def state_space_update(
    input_groups,
    layer_state,
    extra_decay_factor,
    decay_factor,
    angular_frequency,
    step_width,
    input_matrix,
    readout_matrix,
):
    half_width = input_matrix.shape[-1] // 2
    decay_factor = decay_factor.reshape(-1, half_width)
    angular_frequency = angular_frequency.reshape(-1, half_width)
    discrete_real, discrete_imaginary, drive_re, drive_im = transition(
        decay_factor, angular_frequency, step_width
    )
    input_real = input_matrix[..., :half_width]
    input_imaginary = input_matrix[..., half_width:]
    driven_input_real = jnp.einsum(
        "tkl,klf->tkf", input_groups, input_real, precision=TOP_PRECISION
    )
    driven_input_imaginary = jnp.einsum(
        "tkl,klf->tkf", input_groups, input_imaginary, precision=TOP_PRECISION
    )
    state_re = layer_state[..., :half_width]
    state_im = layer_state[..., half_width:]
    carried_real = extra_decay_factor[..., None] * discrete_real[None]
    carried_imaginary = extra_decay_factor[..., None] * discrete_imaginary[None]
    updated_real = (
        carried_real * state_re
        - carried_imaginary * state_im
        + drive_re[None] * driven_input_real
        - drive_im[None] * driven_input_imaginary
    )
    updated_imaginary = (
        carried_real * state_im
        + carried_imaginary * state_re
        + drive_re[None] * driven_input_imaginary
        + drive_im[None] * driven_input_real
    )
    readout_rows = jnp.einsum(
        "hzk,dhk->dhz", readout_matrix[..., :half_width], updated_real, precision=TOP_PRECISION
    ) - jnp.einsum(
        "hzk,dhk->dhz", readout_matrix[..., half_width:], updated_imaginary, precision=TOP_PRECISION
    )
    return (readout_rows, jnp.concatenate([updated_real, updated_imaginary], axis=-1))


def single_layer(
    hidden_rows,
    sequence_lengths,
    layer_state,
    norm_scale_rows,
    input_matrix_weight,
    gate_matrix,
    output_matrix_weight,
    decay_factor,
    angular_frequency,
    step_width,
    input_matrix,
    readout_matrix,
    feedthrough_rows,
    extra_decay_rows,
):
    x_float = hidden_rows.astype(jnp.float32)
    square_sums = jnp.sum(x_float * x_float, axis=1)
    scaled_in = (x_float * norm_scale_rows[None, :]).astype(jnp.bfloat16)
    input_part = jnp.dot(scaled_in, input_matrix_weight, preferred_element_type=jnp.float32)
    gate_part = jnp.dot(scaled_in, gate_matrix, preferred_element_type=jnp.float32)
    local_rows = sequence_lengths.shape[0]
    input_sum, gate_sum, mine_squares = (
        lax.psum_scatter(input_part, "dp", scatter_dimension=0, tiled=True),
        lax.psum_scatter(gate_part, "dp", scatter_dimension=0, tiled=True),
        lax.psum_scatter(square_sums, "dp", scatter_dimension=0, tiled=True),
    )
    scale = lax.rsqrt(mine_squares / D + NORM_EPS)[:, None]
    u_vals = (input_sum * scale).astype(jnp.bfloat16)
    gate_vals = (gate_sum * scale).astype(jnp.bfloat16)
    group_count = layer_state.shape[1]
    input_float = u_vals.astype(jnp.float32)
    token_positions = sequence_lengths - 1
    extra_decay_factor = jnp.exp(jnp.take(extra_decay_rows, token_positions, axis=1).T)
    readout_rows, updated_state = state_space_update(
        input_float.reshape(local_rows, group_count, -1),
        layer_state,
        extra_decay_factor,
        decay_factor,
        angular_frequency,
        step_width,
        input_matrix,
        readout_matrix,
    )
    y_vals = jax.nn.gelu(
        readout_rows.reshape(local_rows, -1) + feedthrough_rows[None, :] * input_float
    )
    mixed = (y_vals * jax.nn.sigmoid(gate_vals.astype(jnp.float32))).astype(jnp.bfloat16)
    branch_terms = jnp.dot(
        lax.all_gather(mixed, "dp", axis=0, tiled=True),
        output_matrix_weight,
        preferred_element_type=jnp.float32,
    )
    branch = lax.psum(branch_terms, "tp").astype(jnp.bfloat16)
    x_next = (x_float + branch.astype(jnp.float32)).astype(jnp.bfloat16)
    return (x_next, updated_state)


def on_device(
    tokens,
    sequence_lengths,
    recurrent_state,
    norm_weight,
    input_weight,
    gate_weight,
    output_weight,
    negated_real_rate,
    frequency,
    discrete_step,
    group_input_matrix,
    group_output_matrix,
    feedthrough_weight,
    extra_log_decay,
):
    hidden_rows = tokens
    states = []
    for index_of_layer in range(STACKED_LAYERS):
        hidden_rows, updated_state = single_layer(
            hidden_rows,
            sequence_lengths,
            recurrent_state[index_of_layer],
            norm_weight[index_of_layer],
            input_weight[index_of_layer],
            gate_weight[index_of_layer],
            output_weight[index_of_layer],
            negated_real_rate[index_of_layer],
            frequency[index_of_layer],
            discrete_step[index_of_layer],
            group_input_matrix[index_of_layer],
            group_output_matrix[index_of_layer],
            feedthrough_weight[index_of_layer],
            extra_log_decay[index_of_layer],
        )
        states.append(updated_state)
    return (hidden_rows, jnp.stack(states, axis=0))


def solution(mesh):
    in_specs = (
        P("grp", "dp"),
        P(("grp", "dp")),
        P(None, ("grp", "dp"), "tp", None),
        P(None, "dp"),
        P(None, "dp", "tp"),
        P(None, "dp", "tp"),
        P(None, "tp", "dp"),
        P(None, "tp"),
        P(None, "tp"),
        P(None, "tp"),
        P(None, "tp", None, None),
        P(None, "tp", None, None),
        P(None, "tp"),
        P(None, "tp", None),
    )
    out_specs = (P("grp", "dp"), P(None, ("grp", "dp"), "tp", None))
    return jax.shard_map(
        on_device, mesh=mesh, in_specs=in_specs, out_specs=out_specs, check_vma=False
    )
```

profile of v0, /device:TPU:0, one launch (start us, length us, event | category | flops | bytes accessed | tf_op | source)
XLA Modules:
  0.0 220.5 jit_solution(5358436251447161086)
XLA Ops:
  8.0 2.6 %fusion.28 = f32[256,512]{1,0:T(8,128)} fusion(bf16[2,1024,512]{2,1,0:T(8,128)(2,1)} %param.20, bf16[256,1024]{1,0:T(8,128)(2,1)} %param.16, f32[1024]{0:T(1024)S(1)} %bitcast.103), kind=kOutput, calls=%fused_computation.51 | convolution fusion | flops 269221888 | bytes 2101248 | tf_op jit(solution)/shard_map/dot_general | solution.py:95
  10.8 2.6 %fusion.26 = f32[256,512]{1,0:T(8,128)} fusion(bf16[2,1024,512]{2,1,0:T(8,128)(2,1)} %param.21, bf16[256,1024]{1,0:T(8,128)(2,1)S(1)} %copy-done.3, f32[1024]{0:T(1024)S(1)} %bitcast.104), kind=kOutput, calls=%fused_computation.49 | convolution fusion | flops 269221888 | bytes 2101248 | tf_op jit(solution)/shard_map/dot_general | solution.py:96
  13.6 8.5 %all-reduce = f32[256]{0:T(256)S(1)} all-reduce(f32[256]{0:T(256)S(1)} %fusion.13), channel_id=3, replica_groups=mesh['grp'=2,'tp'=4,'dp'=4] {'dp'}, use_global_device_ids=true, to_apply=%region_2.4.clone | all-reduce | flops 256 | bytes 2048
  24.1 1.6 copy.53
  25.8 1.9 copy.51
  28.3 2.3 %gather_fusion = f32[64,32]{1,0:T(8,128)S(1)} fusion(f32[32,4096]{0,1:T(8,128)} %bitcast.92, s32[1024]{0:T(1024)S(1)} %pad_clamp_fusion), kind=kCustom, calls=%fused_computation.clone | custom fusion | bytes 16640 | tf_op jit(solution)/shard_map/jit(_take)/gather | solution.py:109
  30.7 1.7 fusion.83
  33.8 2.5 %copy_bitcast_fusion = (f32[64,32,128]{2,0,1:T(8,128)}, f32[64,32,128]{2,0,1:T(8,128)}) fusion(f32[1,64,32,128]{3,2,1,0:T(8,128)S(1)} %get-tuple-element.21, f32[1,64,32,128]{3,2,1,0:T(8,128)S(1)} %get-tuple-element.22), kind=kLoop, calls=%fused_computation.39 | loop fusion | bytes 4194304 | tf_op jit(solution)/shard_map/squeeze | solution.py:156
  36.5 1.0 multiply_convert_fusion.3
  38.5 2.8 %fusion.5 = (f32[64,32,64]{2,0,1:T(8,128)S(1)}, f32[64,32,64]{2,0,1:T(8,128)S(1)}) fusion(f32[32,64,64]{2,1,0:T(8,128)S(1)} %fusion.50, f32[64,32,128]{2,0,1:T(8,128)} %get-tuple-element.46, f32[32,64]{1,0:T(8,128)S(1)} %get-tuple-element.36, f32[32,64]{1,0:T(8,128)S(1)} %get-tuple-element.35, f32[32,64]{1,0:T(8,128)S(1)} %get-tuple-element.34, ...), kind=kOutput, calls=%fused_computation.24 | convolution fusion | flops 27262976 | bytes 2990080 | tf_op jit(solution)/shard_map/tkl,klf->tkf/dot_general | solution.py:46
  41.3 1.7 fusion.48
  43.0 1.8 convolution_subtract_fusion.1
  45.0 14.7 %reduce-scatter.7.cloned.1.call-done = f32[64,512]{1,0:T(8,128)} async-done(((f32[256,512]{1,0:T(8,128)}), f32[64,512]{1,0:T(8,128)}) %reduce-scatter.7.cloned.1.call-update) | async-done | bytes 131088 | tf_op jit(solution)/shard_map/reduce_scatter | solution.py:100
  59.6 1.1 fusion.62
  60.7 5.8 %all_gather.6 = bf16[256,512]{1,0:T(8,128)(2,1)S(1)} all-gather(bf16[64,512]{1,0:T(8,128)(2,1)S(1)} %fusion.62), channel_id=1, replica_groups=mesh['grp'=2,'tp'=4,'dp'=4] {'dp'}, dimensions={0}, use_global_device_ids=true | all-gather | bytes 327680 | tf_op jit(solution)/shard_map/all_gather | solution.py:125
  66.5 1.7 fusion.24
  68.1 44.3 %all-reduce.4 = bf16[256,1024]{1,0:T(8,128)(2,1)} all-reduce(f32[256,1024]{1,0:T(8,128)S(1)} %fusion.24), channel_id=1, replica_groups=mesh['grp'=2,'tp'=4,'dp'=4] {'tp'}, use_global_device_ids=true, to_apply=%region_4.0 | all-reduce | flops 262144 | bytes 1572864 | tf_op jit(solution)/shard_map/psum | solution.py:129
  112.4 1.5 fusion.16
  113.9 2.7 %fusion.22 = f32[256,512]{1,0:T(8,128)} fusion(bf16[2,1024,512]{2,1,0:T(8,128)(2,1)} %param.20, bf16[256,1024]{1,0:T(8,128)(2,1)S(1)} %get-tuple-element.14, f32[1024]{0:T(1024)S(1)} %bitcast.101), kind=kOutput, calls=%fused_computation.45 | convolution fusion | flops 269221888 | bytes 2101248 | tf_op jit(solution)/shard_map/dot_general | solution.py:95
  117.1 6.1 %all-reduce.1 = f32[256]{0:T(256)S(1)} all-reduce(f32[256]{0:T(256)S(1)} %get-tuple-element.13), channel_id=6, replica_groups=mesh['grp'=2,'tp'=4,'dp'=4] {'dp'}, use_global_device_ids=true, to_apply=%region_7.9.clone | all-reduce | flops 256 | bytes 2048
  123.6 1.2 copy-done.15
  124.9 1.2 fusion.20
  126.2 10.6 %reduce-scatter.9.cloned.1.call-done = f32[64,512]{1,0:T(8,128)} async-done(((f32[256,512]{1,0:T(8,128)}), f32[64,512]{1,0:T(8,128)}) %reduce-scatter.9.cloned.1.call-update) | async-done | bytes 131088 | tf_op jit(solution)/shard_map/reduce_scatter | solution.py:99
  138.7 1.5 fusion.11
  140.7 2.5 %copy.50 = f32[2,64,32,128]{3,2,1,0:T(8,128)} copy(f32[2,64,32,128]{3,1,2,0:T(8,128)S(1)} %pad_maximum_fusion) | data formatting | bytes 4194304
  143.3 1.7 fusion.41
  145.0 1.8 convolution_subtract_fusion
  147.0 13.8 %reduce-scatter.11.cloned.1.call-done = f32[64,512]{1,0:T(8,128)} async-done(((f32[256,512]{1,0:T(8,128)}), f32[64,512]{1,0:T(8,128)}) %reduce-scatter.11.cloned.1.call-update) | async-done | bytes 131088 | tf_op jit(solution)/shard_map/reduce_scatter | solution.py:100
  160.8 1.1 fusion.71
  161.9 5.8 %all_gather.7 = bf16[256,512]{1,0:T(8,128)(2,1)S(1)} all-gather(bf16[64,512]{1,0:T(8,128)(2,1)S(1)} %fusion.71), channel_id=1, replica_groups=mesh['grp'=2,'tp'=4,'dp'=4] {'dp'}, dimensions={0}, use_global_device_ids=true | all-gather | bytes 327680 | tf_op jit(solution)/shard_map/all_gather | solution.py:125
  168.1 43.9 %all-reduce.5 = bf16[256,1024]{1,0:T(8,128)(2,1)S(1)} all-reduce(f32[256,1024]{1,0:T(8,128)S(1)} %fusion.18), channel_id=1, replica_groups=mesh['grp'=2,'tp'=4,'dp'=4] {'tp'}, use_global_device_ids=true, to_apply=%region_9.11 | all-reduce | flops 262144 | bytes 1572864 | tf_op jit(solution)/shard_map/psum | solution.py:129
  212.0 2.0 fusion.17
  (78 shorter events, 9.8 us)
Async XLA Ops:
  7.2 3.6 %copy-start.3 = (bf16[256,1024]{1,0:T(8,128)(2,1)S(1)}, bf16[256,1024]{1,0:T(8,128)(2,1)}, u32[]{:S(2)}) copy-start(bf16[256,1024]{1,0:T(8,128)(2,1)} %param.16) | copy-start | bytes 1572868
  7.2 29.4 %reduce-scatter.5.cloned.1.call-start = ((), (), s32[]{:S(2)}) async-start(), calls=%async_computation.4 | async-start | bytes 655360 | tf_op jit(solution)/shard_map/reduce_scatter | solution.py:99
  10.6 11.5 %copy-start.16 = (s32[64]{0:T(128)S(1)}, s32[64]{0:T(128)}, u32[]{:S(2)}) copy-start(s32[64]{0:T(128)} %param.17) | copy-start | bytes 772
  10.6 11.5 %copy-start.14 = (f32[2,32]{1,0:T(2,128)S(1)}, f32[2,32]{1,0:T(2,128)}, u32[]{:S(2)}) copy-start(f32[2,32]{1,0:T(2,128)} %param.25) | copy-start | bytes 772
  10.6 11.5 %copy-start.13 = (f32[2,512]{1,0:T(2,128)S(1)}, f32[2,512]{1,0:T(2,128)}, u32[]{:S(2)}) copy-start(f32[2,512]{1,0:T(2,128)} %param.28) | copy-start | bytes 12292
  10.6 11.6 %copy-start.11 = (f32[2,2048]{1,0:T(2,128)S(1)}, f32[2,2048]{1,0:T(2,128)}, u32[]{:S(2)}) copy-start(f32[2,2048]{1,0:T(2,128)} %param.24) | copy-start | bytes 49156
  10.7 11.6 %copy-start.12 = (f32[2,2048]{1,0:T(2,128)S(1)}, f32[2,2048]{1,0:T(2,128)}, u32[]{:S(2)}) copy-start(f32[2,2048]{1,0:T(2,128)} %param.23) | copy-start | bytes 49156
  10.7 11.8 %copy-start.7 = (f32[2,32,16,128]{3,2,1,0:T(8,128)S(1)}, f32[2,32,16,128]{3,2,1,0:T(8,128)}, u32[]{:S(2)}) copy-start(f32[2,32,16,128]{3,2,1,0:T(8,128)} %param.26) | copy-start | bytes 1572868
  10.7 12.5 %copy-start.8 = (f32[2,32,16,128]{3,2,1,0:T(8,128)S(1)}, f32[2,32,16,128]{3,2,1,0:T(8,128)}, u32[]{:S(2)}) copy-start(f32[2,32,16,128]{3,2,1,0:T(8,128)} %param.27) | copy-start | bytes 1572868
  10.7 48.9 %reduce-scatter.7.cloned.1.call-start = ((), (), s32[]{:S(2)}) async-start(), calls=%async_computation.5 | async-start | bytes 655360 | tf_op jit(solution)/shard_map/reduce_scatter | solution.py:100
  13.4 9.9 %copy-start.4 = (f32[2,32,4096]{2,1,0:T(8,128)S(1)}, f32[2,32,4096]{2,1,0:T(8,128)}, u32[]{:S(2)}) copy-start(f32[2,32,4096]{2,1,0:T(8,128)} %param.29) | copy-start | bytes 3145732
  13.4 123.4 %reduce-scatter.9.cloned.1.call-start = ((), (), s32[]{:S(2)}) async-start(), calls=%async_computation.6 | async-start | bytes 655360 | tf_op jit(solution)/shard_map/reduce_scatter | solution.py:99
  30.7 1.8 copy-start.17
  41.3 18.3 %copy-start.9 = (f32[64,512]{1,0:T(8,128)S(1)}, f32[64,512]{1,0:T(8,128)}, u32[]{:S(2)}) copy-start(f32[64,512]{1,0:T(8,128)} %reduce-scatter.5.cloned.1.call-done) | copy-start | bytes 393220
  113.9 9.3 %copy-start.1 = (bf16[256,1024]{1,0:T(8,128)(2,1)}, bf16[256,1024]{1,0:T(8,128)(2,1)S(1)}, u32[]{:S(2)}) copy-start(bf16[256,1024]{1,0:T(8,128)(2,1)S(1)} %get-tuple-element.14) | copy-start | bytes 1572868
  116.6 44.2 %reduce-scatter.11.cloned.1.call-start = ((), (), s32[]{:S(2)}) async-start(), calls=%async_computation.7 | async-start | bytes 655360 | tf_op jit(solution)/shard_map/reduce_scatter | solution.py:100
  123.2 1.6 copy-start.15
  123.3 1.6 copy-start.2
  124.9 13.0 %copy-start.6 = (f32[32,16,128]{2,1,0:T(8,128)S(1)}, f32[32,16,128]{2,1,0:T(8,128)}, u32[]{:S(2)}) copy-start(f32[32,16,128]{2,1,0:T(8,128)} %get-tuple-element.27) | copy-start | bytes 786436
  124.9 13.8 %copy-start.5 = (f32[64,32,128]{2,0,1:T(8,128)S(1)}, f32[64,32,128]{2,0,1:T(8,128)}, u32[]{:S(2)}) copy-start(f32[64,32,128]{2,0,1:T(8,128)} %get-tuple-element.45) | copy-start | bytes 3145732
  143.3 17.5 %copy-start.10 = (f32[64,512]{1,0:T(8,128)S(1)}, f32[64,512]{1,0:T(8,128)}, u32[]{:S(2)}) copy-start(f32[64,512]{1,0:T(8,128)} %reduce-scatter.9.cloned.1.call-done) | copy-start | bytes 393220
  143.3 24.3 %copy-start = (bf16[2,512,1024]{2,1,0:T(8,128)(2,1)S(1)}, bf16[2,512,1024]{2,1,0:T(8,128)(2,1)}, u32[]{:S(2)}) copy-start(bf16[2,512,1024]{2,1,0:T(8,128)(2,1)} %param.22) | copy-start | bytes 6291460
Sparse Core Ops, SparseCore 0:
  11.0 24.3 reduce-scatter.4
  38.0 21.6 reduce-scatter.6
  116.7 20.0 reduce-scatter.8
  139.1 21.6 reduce-scatter.10
where the time goes:
time: 221 us
  blocking collectives  114 us (52%)
  waiting for transfers between devices  39.2 us (18%)
  matrix products  24.2 us (11%)
  local copies, waits for them, and re-layouts  18.5 us (8%)
  between operations  14.8 us (7%)
  other arithmetic  9.38 us (4%)
    psum x2, blocking collectives, single_layer(): branch = lax.psum(branch_terms, 'tp').astype(jnp.bfloat16)  88.2 us
    reduce_scatter x2, waiting for transfers between devices, single_layer(): lax.psum_scatter(gate_part, 'dp', scatter_dimension=0, tiled=True)  28.5 us
    unnamed x2, blocking collectives  14.7 us
    all_gather x2, blocking collectives, single_layer(): lax.all_gather(mixed, 'dp', axis=0, tiled=True)  11.6 us
    reduce_scatter x2, waiting for transfers between devices, single_layer(): lax.psum_scatter(input_part, 'dp', scatter_dimension=0, tiled=True)  10.6 us
    unnamed x40, local copies, waits for them, and re-layouts  8.03 us
    dot_general x2, matrix products, single_layer(): jnp.dot(scaled_in, input_matrix_weight, preferred_element_type=jnp.float32)  5.29 us
  transfers between devices with their start and end apart: 4, of which 3 were waited for; matrix products, arithmetic and copies ran while one was open for 17% of the time, Pallas kernels for 0%

commit v1 on v0

v1 whole, which is shorter than its diff:
```python
import functools

import jax
import jax.numpy as jnp
from jax import lax
from jax.experimental import pallas as pl
from jax.experimental.pallas import tpu as pltpu
from jax.sharding import PartitionSpec as P

NORM_EPS = 1e-06
MESH = pl.DeviceIdType.MESH
F32 = jnp.float32
BF16 = jnp.bfloat16
CHUNK_ROWS = 16
GELU_SLOPE = 0.7978845608028654

STAGE_AT = (0.0, 4.0, 8.0, 11.0, 16.0)
LAYER_AT = 20.0
CHUNK_AT = 3.0


def dot(a, b, contract=((1,), (0,)), precision=None):
    return lax.dot_general(
        a, b, (contract, ((), ())), preferred_element_type=F32, precision=precision
    )


def iota(shape, axis):
    return lax.broadcasted_iota(jnp.int32, shape, axis)


def expm1(x):
    p = jnp.full_like(x, 1.0 / 39916800.0)
    for d in (3628800.0, 362880.0, 40320.0, 5040.0, 720.0, 120.0, 24.0, 6.0, 2.0, 1.0):
        p = p * x + 1.0 / d
    return p * x


def column_of(row):
    n = row.shape[1]
    eye = iota((n, n), 0) == iota((n, n), 1)
    return jnp.sum(jnp.where(eye, row, 0.0), axis=1, keepdims=True)


def kernel(
    sizes,
    tok_ref,
    len_ref,
    state_ref,
    norm_ref,
    win_ref,
    wgate_ref,
    wout_ref,
    rate_ref,
    freq_ref,
    step_ref,
    gin_ref,
    gout_ref,
    feed_ref,
    decay_ref,
    out_tok,
    out_state,
    xs,
    st,
    norm,
    win,
    wgate,
    wout,
    rate,
    freq,
    step,
    gin,
    gout,
    feed,
    decay,
    kb,
    rb,
    pay,
    got,
    zb,
    part,
    own,
    ab,
    load_sem,
    rs_send,
    rs_recv,
    ag_send,
    ag_recv,
    ar_send,
    ar_recv,
    x_send,
    x_recv,
    out_sem,
):
    layers, dp, tp, chunks, rows, features = sizes
    groups, width = st.shape[2], st.shape[3]
    half = width // 2
    channels = win.shape[2]
    per_group = channels // groups
    blocks = groups // 8
    span = 8 * per_group
    total = features * dp
    pad = pay.shape[-1] - 2 * channels
    me = lax.axis_index("dp")
    z = lax.axis_index("tp")
    mid = tp // 2
    left = z < mid
    is_mid = jnp.logical_or(z == mid - 1, z == mid)
    is_end = jnp.logical_or(z == 0, z == tp - 1)
    inner = jnp.where(left, z + 1, z - 1)
    outer = jnp.where(left, z - 1, z + 1)
    peers = [lax.rem(me + k, dp) for k in range(1, dp)]

    loads = {}

    def load(name, src, dst):
        c = pltpu.make_async_copy(src, dst, load_sem.at[len(loads)])
        c.start()
        loads[name] = c

    load("x0", tok_ref.at[:, 0], xs.at[0, 0])
    load("norm", norm_ref, norm)
    load("win0", win_ref.at[0], win.at[0])
    load("wgate0", wgate_ref.at[0], wgate.at[0])
    for j in range(1, chunks):
        load(f"x{j}", tok_ref.at[:, j], xs.at[0, j])
    load("rate", rate_ref, rate)
    load("freq", freq_ref, freq)
    load("step", step_ref, step)
    load("decay", decay_ref, decay)
    load("gin", gin_ref, gin)
    load("gout", gout_ref, gout)
    load("feed", feed_ref, feed)
    load("state0", state_ref.at[0], st.at[0])
    load("wout0", wout_ref.at[0], wout.at[0])
    for l in range(1, layers):
        load(f"state{l}", state_ref.at[l], st.at[l])
        load(f"win{l}", win_ref.at[l], win.at[l])
        load(f"wgate{l}", wgate_ref.at[l], wgate.at[l])
        load(f"wout{l}", wout_ref.at[l], wout.at[l])
    waited = set()

    def need(*names):
        for name in names:
            if name not in waited:
                waited.add(name)
                loads[name].wait()

    barrier = pltpu.get_barrier_semaphore()
    for p in peers:
        pl.semaphore_signal(barrier, inc=1, device_id={"dp": p}, device_id_type=MESH)
    pl.semaphore_signal(barrier, inc=1, device_id={"tp": inner}, device_id_type=MESH)

    @pl.when(jnp.logical_not(is_end))
    def _():
        pl.semaphore_signal(barrier, inc=1, device_id={"tp": outer}, device_id_type=MESH)

    pl.semaphore_wait(barrier, dp - 1 + jnp.where(is_end, 1, 2))

    def remote(src, dst, send, recv, axis, peer):
        return pltpu.make_async_remote_copy(
            src_ref=src,
            dst_ref=dst,
            send_sem=send,
            recv_sem=recv,
            device_id={axis: peer},
            device_id_type=MESH,
        )

    def rs_copy(l, j, k):
        return remote(
            pay.at[l, j, peers[k]], got.at[l, j, k], rs_send.at[l, j, k], rs_recv.at[l, j, k], "dp", peers[k]
        )

    def ag_copy(l, j, k):
        return remote(
            zb.at[l, j, me], zb.at[l, j, me], ag_send.at[l, j, k], ag_recv.at[l, j, k], "dp", peers[k]
        )

    def ag_arrival(l, j, k):
        origin = lax.rem(me + dp - (k + 1), dp)
        return remote(
            zb.at[l, j, me], zb.at[l, j, origin], ag_send.at[l, j, k], ag_recv.at[l, j, k], "dp", peers[k]
        )

    def sum_copy(l, j):
        slot = jnp.where(is_mid, 1, 0)
        return remote(own.at[l, j], ab.at[l, j, slot], ar_send.at[l, j], ar_recv.at[l, j, slot], "tp", inner)

    def sum_arrival(l, j, slot):
        return remote(own.at[l, j], ab.at[l, j, slot], ar_send.at[l, j], ar_recv.at[l, j, slot], "tp", inner)

    def x_copy(l, j):
        return remote(xs.at[l + 1, j], xs.at[l + 1, j], x_send.at[l, j], x_recv.at[l, j], "tp", outer)

    def state_copy(l, j):
        r = pl.ds(j * rows, rows)
        return pltpu.make_async_copy(st.at[l, r], out_state.at[l, r], out_sem.at[0, l, j])

    def token_copy(j):
        return pltpu.make_async_copy(xs.at[layers, j], out_tok.at[:, j], out_sem.at[1, 0, j])

    mask = (iota((1, 8, span), 2) // per_group) == iota((1, 8, span), 1)

    def prepare_tables():
        need("rate", "freq", "step", "gin", "gout")
        wide = groups * half
        pick = (iota((groups, wide), 1) // half) == iota((groups, wide), 0)
        sel = ((iota((wide, width), 0) % half) == (iota((wide, width), 1) % half)).astype(F32)
        sign = jnp.where(iota((1, width), 1) < half, 1.0, -1.0)
        tables = []
        for l in range(layers):
            both = jnp.concatenate(
                [jnp.where(pick, rate[l : l + 1], 0.0), jnp.where(pick, freq[l : l + 1], 0.0)], axis=0
            )
            flat = dot(both, sel, precision=lax.Precision.HIGHEST)
            a, w = flat[:groups], flat[groups:]
            dt = column_of(step[l : l + 1])
            log_mag = -a * dt
            turn = w * dt
            magnitude = jnp.exp(log_mag)
            cosine = jnp.cos(turn)
            dre = magnitude * cosine
            dim = magnitude * jnp.sin(turn)
            hs = jnp.sin(0.5 * turn)
            nre = expm1(log_mag) * cosine - 2.0 * hs * hs
            den = a * a + w * w
            kre = (-nre * a + dim * w) / den
            kim = (-dim * a - nre * w) / den
            b = gin[l]
            rolled = pltpu.roll(b.reshape(groups * per_group, width), half, 1).reshape(b.shape)
            kb[l] = (kre[:, None, :] * b - (sign * kim)[:, None, :] * rolled).astype(BF16).reshape(
                groups * per_group, width
            )
            rb[l] = (gout[l] * sign[None]).astype(BF16).reshape(groups * per_group, width)
            tables.append((dre, -sign * dim))
        return tables

    def prepare_state(l, tables, position):
        need(f"state{l}", "decay")
        dre, dim = tables[l]
        lg = decay[l]
        hi = lg.astype(BF16)
        lo = (lg - hi.astype(F32)).astype(BF16)
        e = jnp.exp(dot(position, hi, ((1,), (1,))) + dot(position, lo, ((1,), (1,))))
        seqs = e.shape[0]
        spread = jnp.broadcast_to(e[:, None, :], (seqs, 8, groups))
        for b in range(blocks):
            here = iota((1, 8, groups), 2) == (iota((1, 8, groups), 1) + 8 * b)
            factor = jnp.sum(jnp.where(here, spread, 0.0), axis=-1, keepdims=True)
            g = slice(8 * b, 8 * b + 8)
            s = st[l, :, g, :]
            turned = pltpu.roll(s.reshape(seqs * 8, width), half, 1).reshape(s.shape)
            st[l, :, g, :] = factor * (dre[g][None] * s + dim[g][None] * turned)

    def project(l, j):
        if l == 0:
            need(f"x{j}", "norm")
        need(f"win{l}", f"wgate{l}")
        x = xs[l, j].reshape(dp * rows, features).astype(F32)
        squares = jnp.sum(x * x, axis=1, keepdims=True)
        xg = (x * norm[l : l + 1]).astype(BF16)
        pay[l, j, :, :, :channels] = dot(xg, win[l]).astype(BF16).reshape(dp, rows, channels)
        pay[l, j, :, :, channels : 2 * channels] = dot(xg, wgate[l]).astype(BF16).reshape(dp, rows, channels)
        hi = squares.astype(BF16).astype(F32)
        lane = iota((dp * rows, pad), 1) < pad // 2
        pay[l, j, :, :, 2 * channels :] = (
            jnp.where(lane, hi, squares - hi).astype(BF16).reshape(dp, rows, pad)
        )
        for k in range(dp - 1):
            rs_copy(l, j, k).start()

    def update(l, j):
        for k in range(dp - 1):
            rs_copy(l, j, k).wait_recv()
        acc = pay[l, j, me].astype(F32)
        for k in range(dp - 1):
            acc = acc + got[l, j, k].astype(F32)
        squares = jnp.sum(acc[:, 2 * channels :], axis=1, keepdims=True) * (2.0 / pad)
        scale = lax.rsqrt(squares / total + NORM_EPS)
        u = (acc[:, :channels] * scale).astype(BF16).astype(F32)
        gate = (acc[:, channels : 2 * channels] * scale).astype(BF16).astype(F32)
        r = slice(j * rows, (j + 1) * rows)
        reads = []
        for b in range(blocks):
            ub = u[:, b * span : (b + 1) * span]
            spread = jnp.where(mask, jnp.broadcast_to(ub[:, None, :], (rows, 8, span)), 0.0)
            drive = dot(spread.reshape(rows * 8, span).astype(BF16), kb[l, b * span : (b + 1) * span])
            g = slice(8 * b, 8 * b + 8)
            new = st[l, r, g, :] + drive.reshape(rows, 8, width)
            st[l, r, g, :] = new
            read = dot(
                new.reshape(rows * 8, width).astype(BF16), rb[l, b * span : (b + 1) * span], ((1,), (1,))
            )
            reads.append(jnp.sum(jnp.where(mask, read.reshape(rows, 8, span), 0.0), axis=1))
        state_copy(l, j).start()
        v = (jnp.concatenate(reads, axis=1) if blocks > 1 else reads[0]) + feed[l : l + 1] * u
        y = 0.5 * v * (1.0 + jnp.tanh(GELU_SLOPE * (v + 0.044715 * (v * v * v))))
        zb[l, j, me] = (y / (1.0 + jnp.exp(-gate))).astype(BF16)
        for k in range(dp - 1):
            ag_copy(l, j, k).start()

    def branch(l, j):
        need(f"wout{l}")
        for k in range(dp - 1):
            ag_arrival(l, j, k).wait_recv()
        term = dot(zb[l, j].reshape(dp * rows, channels), wout[l]).reshape(dp, rows, features)

        @pl.when(is_end)
        def _():
            own[l, j] = term.astype(BF16)
            sum_copy(l, j).start()

        @pl.when(jnp.logical_not(is_end))
        def _():
            part[l, j] = term

    def gather_in(l, j):
        @pl.when(jnp.logical_not(is_end))
        def _():
            sum_arrival(l, j, 0).wait_recv()
            own[l, j] = (part[l, j] + ab[l, j, 0].astype(F32)).astype(BF16)
            sum_copy(l, j).start()

    def finish(l, j):
        @pl.when(is_mid)
        def _():
            sum_arrival(l, j, 1).wait_recv()
            both = (own[l, j].astype(F32) + ab[l, j, 1].astype(F32)).astype(BF16)
            xs[l + 1, j] = (xs[l, j].astype(F32) + both.astype(F32)).astype(BF16)

        @pl.when(jnp.logical_not(is_mid))
        def _():
            x_copy(l, j).wait_recv()

        @pl.when(jnp.logical_not(is_end))
        def _():
            x_copy(l, j).start()

        if l == layers - 1:
            token_copy(j).start()

    stages = (project, update, branch, gather_in, finish)
    order = sorted(
        (l * LAYER_AT + STAGE_AT[s] + j * CHUNK_AT, l, s, j)
        for l in range(layers)
        for s in range(len(stages))
        for j in range(chunks)
    )
    tables = None
    prepared = set()
    for at, l, s, j in order:
        if s == 1 and tables is None:
            tables = prepare_tables()
            lengths = len_ref[...]
            places = decay.shape[2]
            position = (iota((lengths.shape[0], places), 1) == lengths - 1).astype(F32).astype(BF16)
            need("feed")
        if s == 1 and not prepared:
            for m in range(layers):
                prepared.add(m)
                prepare_state(m, tables, position)
        stages[s](l, j)

    for l in range(layers):
        for j in range(chunks):
            for k in range(dp - 1):
                rs_copy(l, j, k).wait_send()
                ag_copy(l, j, k).wait_send()
            sum_copy(l, j).wait_send()

            @pl.when(jnp.logical_not(is_end))
            def _():
                x_copy(l, j).wait_send()

            state_copy(l, j).wait()
    for j in range(chunks):
        token_copy(j).wait()


def on_device(
    dp,
    tp,
    tokens,
    sequence_lengths,
    recurrent_state,
    norm_weight,
    input_weight,
    gate_weight,
    output_weight,
    negated_real_rate,
    frequency,
    discrete_step,
    group_input_matrix,
    group_output_matrix,
    feedthrough_weight,
    extra_log_decay,
):
    batch, features = tokens.shape
    mine = sequence_lengths.shape[0]
    rows = CHUNK_ROWS if mine % CHUNK_ROWS == 0 else mine
    chunks = mine // rows
    layers = input_weight.shape[0]
    channels = input_weight.shape[2]
    pad = 128
    tall = 2 * channels + pad
    dma = pltpu.SemaphoreType.DMA
    any_spec = pl.BlockSpec(memory_space=pl.ANY)
    vmem = lambda a: pltpu.VMEM(a.shape, a.dtype)
    piece = (layers, chunks, dp, rows, features)
    n_tab = group_input_matrix.shape[1] * group_input_matrix.shape[2]
    width = group_input_matrix.shape[3]
    tok, state = pl.pallas_call(
        functools.partial(kernel, (layers, dp, tp, chunks, rows, features)),
        out_shape=(
            jax.ShapeDtypeStruct((dp, chunks, rows, features), BF16),
            jax.ShapeDtypeStruct(recurrent_state.shape, F32),
        ),
        in_specs=[any_spec, pl.BlockSpec(memory_space=pltpu.VMEM)] + [any_spec] * 12,
        out_specs=(any_spec, any_spec),
        scratch_shapes=[
            pltpu.VMEM((layers + 1,) + piece[1:], BF16),
            vmem(recurrent_state),
            vmem(norm_weight),
            vmem(input_weight),
            vmem(gate_weight),
            vmem(output_weight),
            vmem(negated_real_rate),
            vmem(frequency),
            vmem(discrete_step),
            vmem(group_input_matrix),
            vmem(group_output_matrix),
            vmem(feedthrough_weight),
            vmem(extra_log_decay),
            pltpu.VMEM((layers, n_tab, width), BF16),
            pltpu.VMEM((layers, n_tab, width), BF16),
            pltpu.VMEM((layers, chunks, dp, rows, tall), BF16),
            pltpu.VMEM((layers, chunks, dp - 1, rows, tall), BF16),
            pltpu.VMEM((layers, chunks, dp, rows, channels), BF16),
            pltpu.VMEM(piece, F32),
            pltpu.VMEM(piece, BF16),
            pltpu.VMEM((layers, chunks, 2, dp, rows, features), BF16),
            dma((9 + chunks + 4 * layers,)),
            dma((layers, chunks, dp - 1)),
            dma((layers, chunks, dp - 1)),
            dma((layers, chunks, dp - 1)),
            dma((layers, chunks, dp - 1)),
            dma((layers, chunks)),
            dma((layers, chunks, 2)),
            dma((layers, chunks)),
            dma((layers, chunks)),
            dma((2, layers, chunks)),
        ],
        compiler_params=pltpu.CompilerParams(
            collective_id=0, has_side_effects=True, vmem_limit_bytes=60 * 1024 * 1024
        ),
    )(
        tokens.reshape(dp, chunks, rows, features),
        sequence_lengths.reshape(mine, 1),
        recurrent_state,
        norm_weight,
        input_weight,
        gate_weight,
        output_weight,
        negated_real_rate,
        frequency,
        discrete_step,
        group_input_matrix,
        group_output_matrix,
        feedthrough_weight,
        extra_log_decay,
    )
    return tok.reshape(batch, features), state


def solution(mesh):
    in_specs = (
        P("grp", "dp"),
        P(("grp", "dp")),
        P(None, ("grp", "dp"), "tp", None),
        P(None, "dp"),
        P(None, "dp", "tp"),
        P(None, "dp", "tp"),
        P(None, "tp", "dp"),
        P(None, "tp"),
        P(None, "tp"),
        P(None, "tp"),
        P(None, "tp", None, None),
        P(None, "tp", None, None),
        P(None, "tp"),
        P(None, "tp", None),
    )
    out_specs = (P("grp", "dp"), P(None, ("grp", "dp"), "tp", None))
    return jax.shard_map(
        functools.partial(on_device, mesh.shape["dp"], mesh.shape["tp"]),
        mesh=mesh,
        in_specs=in_specs,
        out_specs=out_specs,
        check_vma=False,
    )
```

time: 221 us -> 76.5 us (0.35)
  blocking collectives: 114 us -> 0 us
  Pallas kernels: 0 us -> 69.3 us
  waiting for transfers between devices: 39.2 us -> 0 us
  matrix products: 24.2 us -> 0 us
  between operations: 14.8 us -> 0.64 us
  local copies, waits for them, and re-layouts: 18.5 us -> 6.31 us
  other arithmetic: 9.38 us -> 0 us
    psum x2 -> x0, blocking collectives: 88.2 us -> none  [single_layer(): branch = lax.psum(branch_terms, 'tp').astype(jnp.bfloat16)]
    pallas_call x0 -> x1, Pallas kernels: none -> 69.3 us  [on_device(): pl.pallas_call(functools.partial(kernel, (layers, dp, tp, chunks, rows, f...]
    reduce_scatter x4 -> x0, waiting for transfers between devices: 39.1 us -> none  [the longest x2 28.5 us: single_layer(): lax.psum_scatter(gate_part, 'dp', scatter_dimension=0, tiled=True)]
    dot_general x14 -> x0, matrix products: 24.2 us -> none  [the longest x2 5.29 us: single_layer(): jnp.dot(scaled_in, input_matrix_weight, preferred_element_type=jnp.float32)]
    unnamed x2 -> x0, blocking collectives: 14.7 us -> none
    all_gather x2 -> x0, blocking collectives: 11.6 us -> none  [single_layer(): lax.all_gather(mixed, 'dp', axis=0, tiled=True)]
    convert_element_type x5 -> x0, other arithmetic: 6.12 us -> none  [the longest x2 2.12 us: single_layer(): (y_vals * jax.nn.sigmoid(gate_vals.astype(jnp.float32))).astype(jnp.bfloa...]
    slice x5 -> x0, local copies, waits for them, and re-layouts: 3.47 us -> none  [the longest x1 1.74 us: on_device(): recurrent_state[index_of_layer]]
  transfers between devices with their start and end apart: 4 -> 0, of which waited for: 3 -> 0; matrix products, arithmetic and copies ran while one was open for 17% -> 0% of each run, Pallas kernels for 0% -> 0%
where the time goes in v1:
time: 76.5 us; the launch traced here: 76.3 us
  Pallas kernels  69.3 us (91%)
  local copies, waits for them, and re-layouts  6.31 us (8%)
    pallas_call x1, Pallas kernels, on_device(): pl.pallas_call(functools.partial(kernel, (layers, dp, tp, chunks, rows, f...  69.3 us
    unnamed x2, local copies, waits for them, and re-layouts  4.95 us

profile of v1, /device:TPU:0, one launch (start us, length us, event | category | flops | bytes accessed | tf_op | source)
XLA Modules:
  0.0 76.3 jit_solution(6848616222276894446)
XLA Ops:
  0.6 1.4 %copy.16.len_ref = s32[64,1]{1,0:T(8,128)} copy(s32[64,1]{0,1:T(1,128)} %bitcast.5) | data formatting | bytes 512 | tf_op jit(solution)/shard_map/reshape | solution.py:459
  2.0 69.3 %shard_map.149 = (bf16[4,4,16,1024]{3,2,1,0:T(8,128)(2,1)}, f32[2,64,32,128]{3,2,1,0:T(8,128)}) custom-call(bf16[4,4,16,1024]{3,2,1,0:T(8,128)(2,1)} %bitcast.3, s32[64,1]{1,0:T(8,128)} %copy.16.len_ref, f32[2,64,32,128]{3,2,1,0:T(8,128)} %state_ref.1, f32[2,1024]{1,0:T(2,128)} %norm_ref.1, bf16[2,1024,512]{2,1,0:T(8,128)(2,1)} %win_ref.1, ...), custom_call_target="tpu_custom_call" | custom-call | tf_op jit(solution)/shard_map/pallas_call | solution.py:413
  71.3 1.9 %copy.19 = bf16[256,1024]{1,0:T(8,128)(2,1)} copy(bf16[256,1024]{1,0:T(8,128)(2,1)} %bitcast.4) | data formatting | bytes 1048576
  73.2 3.1 %copy.20 = f32[2,64,32,128]{3,2,1,0:T(8,128)} copy(f32[2,64,32,128]{3,2,1,0:T(8,128)} %get-tuple-element.9) | data formatting | bytes 4194304

commit v2 on v1

--- a/solution.py
+++ b/solution.py
@@ -12,11 +12,12 @@
 F32 = jnp.float32
 BF16 = jnp.bfloat16
 CHUNK_ROWS = 16
+PIECES = 4
 GELU_SLOPE = 0.7978845608028654
 
-STAGE_AT = (0.0, 4.0, 8.0, 11.0, 16.0)
-LAYER_AT = 20.0
-CHUNK_AT = 3.0
+STAGE_AT = (0.0, 5.0, 9.5, 14.5, 19.5)
+LAYER_AT = 22.0
+CHUNK_AT = 4.0
 
 
 def dot(a, b, contract=((1,), (0,)), precision=None):
@@ -59,9 +60,9 @@
     feed_ref,
     decay_ref,
     out_tok,
-    out_state,
+    st,
     xs,
-    st,
+    seq,
     norm,
     win,
     wgate,
@@ -90,7 +91,6 @@
     ar_recv,
     x_send,
     x_recv,
-    out_sem,
 ):
     layers, dp, tp, chunks, rows, features = sizes
     groups, width = st.shape[2], st.shape[3]
@@ -124,6 +124,7 @@
     load("wgate0", wgate_ref.at[0], wgate.at[0])
     for j in range(1, chunks):
         load(f"x{j}", tok_ref.at[:, j], xs.at[0, j])
+    load("seq", len_ref, seq)
     load("rate", rate_ref, rate)
     load("freq", freq_ref, freq)
     load("step", step_ref, step)
@@ -183,22 +184,23 @@
             zb.at[l, j, me], zb.at[l, j, origin], ag_send.at[l, j, k], ag_recv.at[l, j, k], "dp", peers[k]
         )
 
-    def sum_copy(l, j):
-        slot = jnp.where(is_mid, 1, 0)
-        return remote(own.at[l, j], ab.at[l, j, slot], ar_send.at[l, j], ar_recv.at[l, j, slot], "tp", inner)
-
-    def sum_arrival(l, j, slot):
-        return remote(own.at[l, j], ab.at[l, j, slot], ar_send.at[l, j], ar_recv.at[l, j, slot], "tp", inner)
-
-    def x_copy(l, j):
-        return remote(xs.at[l + 1, j], xs.at[l + 1, j], x_send.at[l, j], x_recv.at[l, j], "tp", outer)
-
-    def state_copy(l, j):
-        r = pl.ds(j * rows, rows)
-        return pltpu.make_async_copy(st.at[l, r], out_state.at[l, r], out_sem.at[0, l, j])
-
-    def token_copy(j):
-        return pltpu.make_async_copy(xs.at[layers, j], out_tok.at[:, j], out_sem.at[1, 0, j])
+    pieces = PIECES if dp % PIECES == 0 else 1
+    cuts = [slice(p * dp // pieces, (p + 1) * dp // pieces) for p in range(pieces)]
+
+    def sum_copy(l, j, p, slot=None):
+        slot = jnp.where(is_mid, 1, 0) if slot is None else slot
+        d = pl.ds(p * (dp // pieces), dp // pieces)
+        return remote(
+            own.at[l, j, d], ab.at[l, j, slot, d], ar_send.at[l, j, p], ar_recv.at[l, j, slot, p], "tp", inner
+        )
+
+    def x_copy(l, j, p):
+        d = pl.ds(p * (dp // pieces), dp // pieces)
+        there = after(l, j).at[d]
+        return remote(there, there, x_send.at[l, j, p], x_recv.at[l, j, p], "tp", outer)
+
+    def after(l, j):
+        return xs.at[l + 1, j] if l + 1 < layers else out_tok.at[j]
 
     mask = (iota((1, 8, span), 2) // per_group) == iota((1, 8, span), 1)
 
@@ -293,7 +295,6 @@
                 new.reshape(rows * 8, width).astype(BF16), rb[l, b * span : (b + 1) * span], ((1,), (1,))
             )
             reads.append(jnp.sum(jnp.where(mask, read.reshape(rows, 8, span), 0.0), axis=1))
-        state_copy(l, j).start()
         v = (jnp.concatenate(reads, axis=1) if blocks > 1 else reads[0]) + feed[l : l + 1] * u
         y = 0.5 * v * (1.0 + jnp.tanh(GELU_SLOPE * (v + 0.044715 * (v * v * v))))
         zb[l, j, me] = (y / (1.0 + jnp.exp(-gate))).astype(BF16)
@@ -308,8 +309,9 @@
 
         @pl.when(is_end)
         def _():
-            own[l, j] = term.astype(BF16)
-            sum_copy(l, j).start()
+            for p, d in enumerate(cuts):
+                own[l, j, d] = term[d].astype(BF16)
+                sum_copy(l, j, p).start()
 
         @pl.when(jnp.logical_not(is_end))
         def _():
@@ -318,27 +320,31 @@
     def gather_in(l, j):
         @pl.when(jnp.logical_not(is_end))
         def _():
-            sum_arrival(l, j, 0).wait_recv()
-            own[l, j] = (part[l, j] + ab[l, j, 0].astype(F32)).astype(BF16)
-            sum_copy(l, j).start()
+            for p, d in enumerate(cuts):
+                sum_copy(l, j, p, 0).wait_recv()
+                own[l, j, d] = (part[l, j, d] + ab[l, j, 0, d].astype(F32)).astype(BF16)
+                sum_copy(l, j, p).start()
 
     def finish(l, j):
         @pl.when(is_mid)
         def _():
-            sum_arrival(l, j, 1).wait_recv()
-            both = (own[l, j].astype(F32) + ab[l, j, 1].astype(F32)).astype(BF16)
-            xs[l + 1, j] = (xs[l, j].astype(F32) + both.astype(F32)).astype(BF16)
+            for p, d in enumerate(cuts):
+                sum_copy(l, j, p, 1).wait_recv()
+                both = (own[l, j, d].astype(F32) + ab[l, j, 1, d].astype(F32)).astype(BF16)
+                after(l, j)[d] = (xs[l, j, d].astype(F32) + both.astype(F32)).astype(BF16)
+
+                @pl.when(jnp.logical_not(is_end))
+                def _():
+                    x_copy(l, j, p).start()
 
         @pl.when(jnp.logical_not(is_mid))
         def _():
-            x_copy(l, j).wait_recv()
-
-        @pl.when(jnp.logical_not(is_end))
-        def _():
-            x_copy(l, j).start()
-
-        if l == layers - 1:
-            token_copy(j).start()
+            for p, d in enumerate(cuts):
+                x_copy(l, j, p).wait_recv()
+
+                @pl.when(jnp.logical_not(is_end))
+                def _():
+                    x_copy(l, j, p).start()
 
     stages = (project, update, branch, gather_in, finish)
     order = sorted(
@@ -348,17 +354,15 @@
         for j in range(chunks)
     )
     tables = None
-    prepared = set()
     for at, l, s, j in order:
         if s == 1 and tables is None:
             tables = prepare_tables()
-            lengths = len_ref[...]
+            need("seq")
+            lengths = column_of(seq[...].astype(F32)).astype(jnp.int32)
             places = decay.shape[2]
             position = (iota((lengths.shape[0], places), 1) == lengths - 1).astype(F32).astype(BF16)
             need("feed")
-        if s == 1 and not prepared:
             for m in range(layers):
-                prepared.add(m)
                 prepare_state(m, tables, position)
         stages[s](l, j)
 
@@ -367,15 +371,13 @@
             for k in range(dp - 1):
                 rs_copy(l, j, k).wait_send()
                 ag_copy(l, j, k).wait_send()
-            sum_copy(l, j).wait_send()
+            for p in range(pieces):
+                sum_copy(l, j, p).wait_send()
 
             @pl.when(jnp.logical_not(is_end))
             def _():
-                x_copy(l, j).wait_send()
-
-            state_copy(l, j).wait()
-    for j in range(chunks):
-        token_copy(j).wait()
+                for p in range(pieces):
+                    x_copy(l, j, p).wait_send()
 
 
 def on_device(
@@ -413,14 +415,14 @@
     tok, state = pl.pallas_call(
         functools.partial(kernel, (layers, dp, tp, chunks, rows, features)),
         out_shape=(
-            jax.ShapeDtypeStruct((dp, chunks, rows, features), BF16),
-            jax.ShapeDtypeStruct(recurrent_state.shape, F32),
+            pltpu.VMEM((chunks, dp, rows, features), BF16),
+            pltpu.VMEM(recurrent_state.shape, F32),
         ),
-        in_specs=[any_spec, pl.BlockSpec(memory_space=pltpu.VMEM)] + [any_spec] * 12,
-        out_specs=(any_spec, any_spec),
+        in_specs=[any_spec] * 14,
+        out_specs=(pl.BlockSpec(memory_space=pltpu.VMEM),) * 2,
         scratch_shapes=[
-            pltpu.VMEM((layers + 1,) + piece[1:], BF16),
-            vmem(recurrent_state),
+            pltpu.VMEM(piece, BF16),
+            pltpu.VMEM((1, mine), jnp.int32),
             vmem(norm_weight),
             vmem(input_weight),
             vmem(gate_weight),
@@ -440,23 +442,22 @@
             pltpu.VMEM(piece, F32),
             pltpu.VMEM(piece, BF16),
             pltpu.VMEM((layers, chunks, 2, dp, rows, features), BF16),
-            dma((9 + chunks + 4 * layers,)),
+            dma((10 + chunks + 4 * layers,)),
             dma((layers, chunks, dp - 1)),
             dma((layers, chunks, dp - 1)),
             dma((layers, chunks, dp - 1)),
             dma((layers, chunks, dp - 1)),
-            dma((layers, chunks)),
-            dma((layers, chunks, 2)),
-            dma((layers, chunks)),
-            dma((layers, chunks)),
-            dma((2, layers, chunks)),
+            dma((layers, chunks, PIECES)),
+            dma((layers, chunks, 2, PIECES)),
+            dma((layers, chunks, PIECES)),
+            dma((layers, chunks, PIECES)),
         ],
         compiler_params=pltpu.CompilerParams(
-            collective_id=0, has_side_effects=True, vmem_limit_bytes=60 * 1024 * 1024
+            collective_id=0, has_side_effects=True, vmem_limit_bytes=61 * 1024 * 1024
         ),
     )(
         tokens.reshape(dp, chunks, rows, features),
-        sequence_lengths.reshape(mine, 1),
+        sequence_lengths.reshape(1, mine),
         recurrent_state,
         norm_weight,
         input_weight,
@@ -470,7 +471,7 @@
         feedthrough_weight,
         extra_log_decay,
     )
-    return tok.reshape(batch, features), state
+    return tok.transpose(1, 0, 2, 3).reshape(batch, features), state
 
 
 def solution(mesh):

time: 76.5 us -> 63.8 us (0.83)
  Pallas kernels: 69.3 us -> 60.8 us
  local copies, waits for them, and re-layouts: 6.31 us -> 2.16 us
    pallas_call x1, Pallas kernels: 69.3 us -> 60.8 us  [on_device(): pl.pallas_call(functools.partial(kernel, (layers, dp, tp, chunks, rows, f...]
    unnamed x2 -> x1, local copies, waits for them, and re-layouts: 4.95 us -> 1.32 us
    reshape x1 -> x0, local copies, waits for them, and re-layouts: 1.36 us -> none  [on_device(): sequence_lengths.reshape(mine, 1)]
    transpose x0 -> x1, local copies, waits for them, and re-layouts: none -> 0.84 us  [on_device(): return (tok.transpose(1, 0, 2, 3).reshape(batch, features), state)]
where the time goes in v2:
time: 63.8 us; the launch traced here: 63.6 us
  Pallas kernels  60.8 us (95%)
  local copies, waits for them, and re-layouts  2.16 us (3%)
  between operations  0.64 us (1%)
    pallas_call x1, Pallas kernels, on_device(): pl.pallas_call(functools.partial(kernel, (layers, dp, tp, chunks, rows, f...  60.8 us
    unnamed x1, local copies, waits for them, and re-layouts  1.32 us

profile of v2, /device:TPU:0, one launch (start us, length us, event | category | flops | bytes accessed | tf_op | source)
XLA Modules:
  0.0 63.6 jit_solution(1236571494439314934)
XLA Ops:
  0.6 60.8 %shard_map.149 = (bf16[4,4,16,1024]{3,2,1,0:T(8,128)(2,1)S(1)}, f32[2,64,32,128]{3,2,1,0:T(8,128)S(1)}) custom-call(bf16[4,4,16,1024]{3,2,1,0:T(8,128)(2,1)} %bitcast.5, s32[1,64]{1,0:T(1,128)} %bitcast.7, f32[2,64,32,128]{3,2,1,0:T(8,128)} %state_ref.1, f32[2,1024]{1,0:T(2,128)} %norm_ref.1, bf16[2,1024,512]{2,1,0:T(8,128)(2,1)} %win_ref.1, ...), custom_call_target="tpu_custom_call" | custom-call | tf_op jit(solution)/shard_map/pallas_call | solution.py:415
  61.5 0.8 %copy.16 = bf16[4,4,16,1024]{3,2,1,0:T(8,128)(2,1)} copy(bf16[4,4,16,1024]{3,2,0,1:T(8,128)(2,1)S(1)} %bitcast.4) | data formatting | bytes 1048576 | tf_op jit(solution)/shard_map/transpose | solution.py:474
  62.3 1.3 %copy.18 = f32[2,64,32,128]{3,2,1,0:T(8,128)} copy(f32[2,64,32,128]{3,2,1,0:T(8,128)S(1)} %get-tuple-element.7) | data formatting | bytes 4194304
